TPU v7x, 32 devices: a whole 2x2x4 slice. The times are simulated.
32 devices in a mesh: sp: 8 (over z, core), tp: 4 (over y, x).
Axes of the slice: x: 2, y: 2, z: 4, core: 2. Of those that a mesh axis runs over, the one named last changes fastest.
Arguments:
- moe_input: bfloat16 [2048, 2048], P('sp', 'tp'), may hold values from -6 to 6
- out_grad: bfloat16 [2048, 2048], P('sp', 'tp'), may hold values from -8 to 8
- routes: int32 [2048, 2], P('sp'), may hold values from 0 to 7, all different within a row; in each aligned block of 256 rows (0 to 255, 256 to 511, ...) at most 80 rows name the same one
- route_weight: float32 [2048, 2], P('sp'), may hold values from 0.2 to 1.5
- w_gate: bfloat16 [8, 2048, 2048], P('sp', None, 'tp'), may hold values from -0.125 to 0.125
- w_up: bfloat16 [8, 2048, 2048], P('sp', None, 'tp'), may hold values from -0.125 to 0.125
- w_down: bfloat16 [8, 2048, 2048], P('sp', 'tp'), may hold values from -0.125 to 0.125
- w_out: bfloat16 [2048, 2048], P(None, 'tp'), may hold values from -0.125 to 0.125
- queries: bfloat16 [2048, 1024], P('sp', 'tp'), may hold values from -6 to 6
- key_rows: bfloat16 [2048, 1024], P('sp', 'tp'), may hold values from -6 to 6
- value_rows: bfloat16 [2048, 2048], P('sp', 'tp'), may hold values from -6 to 6
- log_decay: float32 [2048, 1024], P('sp', 'tp'), may hold values from -1 to 0
Outputs:
- grad_gate: bfloat16 [8, 2048, 2048], P('sp', None, 'tp')
- grad_up: bfloat16 [8, 2048, 2048], P('sp', None, 'tp')
- grad_down: bfloat16 [8, 2048, 2048], P('sp', 'tp')
- grad_proj: float32 [2048, 2048], P('sp', 'tp')
- grad_queries: bfloat16 [2048, 1024], P('sp', 'tp')
- grad_keys: bfloat16 [2048, 1024], P('sp', 'tp')
- grad_values: bfloat16 [2048, 2048], P('sp', 'tp')
- grad_decay: float32 [2048, 1024], P('sp', 'tp')
Inputs may be any that keep to these rules, and one draw needn't show every extreme that they name: `routes`: A token's experts differ. Within each aligned block of 256 tokens no expert is named more than 80 times, and in some block one expert is named exactly 80 times.
All inputs are finite; a program needn't handle non-finite values.
Results may differ from a plain program's by a relative error of at most 0.025.
Values may be sent and summed in bfloat16 or wider, within the bound.
A program may use at most 64 MiB of HBM per device.

v0:
```python
import jax
import jax.numpy as jnp
from jax import lax
from jax.sharding import PartitionSpec as P

KEY_CHANNELS = 32
VAL_DIM = 64
TOP = 2
BLOCK = 64


PRECISE = lax.Precision.HIGHEST


def carried_in(value, axis, join, neutral, backward):
    count, mine = (lax.axis_size(axis), lax.axis_index(axis))
    pieces = jax.tree.map(lambda part: lax.all_gather(part, axis), value)
    if backward:
        pieces = jax.tree.map(lambda part: part[::-1], pieces)
        mine = count - 1 - mine
    subtotal = jax.tree.map(
        lambda part, zero: jnp.full_like(part, 0) + jnp.asarray(zero, part.dtype), value, neutral
    )

    def hop(position, subtotal):
        longer = join(subtotal, jax.tree.map(lambda part: part[position], pieces))
        return jax.tree.map(lambda new, old: jnp.where(position < mine, new, old), longer, subtotal)

    return lax.fori_loop(0, count - 1, hop, subtotal)


def mixer_pass(queries, key_rows, value_rows, log_decay, state_in):
    length = queries.shape[0]
    blocks = length // BLOCK
    nheads = state_in.shape[0]
    query_blocks = queries.reshape(blocks, BLOCK, nheads, KEY_CHANNELS)
    key_blocks = key_rows.reshape(blocks, BLOCK, nheads, KEY_CHANNELS) * KEY_CHANNELS ** (-0.5)
    value_blocks = value_rows.reshape(blocks, BLOCK, nheads, VAL_DIM)
    decays = log_decay.reshape(blocks, BLOCK, nheads, KEY_CHANNELS)
    cumulative = jnp.cumsum(decays, axis=1)
    closing = cumulative[:, -1]
    query_scaled = query_blocks * jnp.exp(cumulative)
    key_scaled = key_blocks * jnp.exp(-cumulative)
    causal = jnp.tril(jnp.ones((BLOCK, BLOCK), jnp.float32))
    scores = jnp.einsum("nthd,nshd->nhts", query_scaled, key_scaled, precision=PRECISE) * causal
    within = jnp.einsum("nhts,nshv->nthv", scores, value_blocks, precision=PRECISE)
    key_tail = key_blocks * jnp.exp(closing[:, None] - cumulative)
    additions = jnp.einsum("nshd,nshv->nhdv", key_tail, value_blocks, precision=PRECISE)

    def advance(state_now, pieces):
        return (jnp.exp(pieces[0])[..., None] * state_now + pieces[1], state_now)

    state_out, entering = lax.scan(advance, state_in, (closing, additions))
    carried = jnp.einsum("nthd,nhdv->nthv", query_scaled, entering, precision=PRECISE)
    return (within + carried).reshape(length, nheads * VAL_DIM)


def carry_terms(key_full, value_full, decay_full):
    length = key_full.shape[0]
    blocks = length // BLOCK
    nheads = key_full.shape[1] // KEY_CHANNELS
    key_blocks = key_full.reshape(blocks, BLOCK, nheads, KEY_CHANNELS) * KEY_CHANNELS ** (-0.5)
    value_blocks = value_full.reshape(blocks, BLOCK, nheads, VAL_DIM)
    cumulative = jnp.cumsum(decay_full.reshape(blocks, BLOCK, nheads, KEY_CHANNELS), axis=1)
    closing = cumulative[:, -1]
    key_tail = key_blocks * jnp.exp(closing[:, None] - cumulative)
    additions = jnp.einsum("nshd,nshv->nhdv", key_tail, value_blocks, precision=PRECISE)
    log_total = jnp.sum(closing, axis=0)
    remaining = log_total[None] - jnp.cumsum(closing, axis=0)
    increment = jnp.einsum("nhd,nhdv->hdv", jnp.exp(remaining), additions, precision=PRECISE)
    return (log_total, increment)


def chain_step(earlier, latter):
    return (earlier[0] + latter[0], jnp.exp(latter[0])[..., None] * earlier[1] + latter[1])


def body(
    moe_input,
    out_grad,
    routes,
    route_weight,
    w_gate,
    w_up,
    w_down,
    w_out,
    queries,
    key_rows,
    value_rows,
    log_decay,
):
    sp_count = lax.axis_size("sp")
    token_count = out_grad.shape[0]
    pair_count = token_count * TOP
    capacity = 5 * token_count * TOP // (4 * sp_count)
    query_full = queries.astype(jnp.float32)
    key_full = key_rows.astype(jnp.float32)
    value_full = value_rows.astype(jnp.float32)
    (log_total, increment), pull_carry = jax.vjp(carry_terms, key_full, value_full, log_decay)
    state_in = carried_in(
        (log_total, increment),
        "sp",
        chain_step,
        (jnp.zeros_like(log_total), jnp.zeros_like(increment)),
        False,
    )[1]
    mixer_raw, pull_mixer = jax.vjp(
        mixer_pass, query_full, key_full, value_full, log_decay, state_in
    )
    mixer_out = mixer_raw.astype(jnp.bfloat16)
    flat_routes = routes.reshape(pair_count)
    onehot = (flat_routes[:, None] == jnp.arange(sp_count, dtype=jnp.int32)[None, :]).astype(
        jnp.int32
    )
    position = jnp.sum((jnp.cumsum(onehot, axis=0) - onehot) * onehot, axis=1)
    pair_slot = flat_routes * capacity + position
    slot_pair = (
        jnp.full((sp_count * capacity,), pair_count, jnp.int32)
        .at[pair_slot]
        .set(jnp.arange(pair_count, dtype=jnp.int32))
    )
    slot_token = slot_pair // TOP
    row_total = sp_count * capacity
    columns = out_grad.shape[1]
    weighted = (route_weight[:, :, None] * out_grad[:, None, :].astype(jnp.float32)).astype(
        jnp.bfloat16
    )
    weighted_pad = jnp.concatenate(
        [weighted.reshape(pair_count, columns), jnp.zeros((1, columns), jnp.bfloat16)], axis=0
    )
    inputs_pad = jnp.concatenate([moe_input, jnp.zeros((1, columns), jnp.bfloat16)], axis=0)
    send_in = jnp.take(inputs_pad, slot_token, axis=0).reshape(sp_count, capacity, columns)
    send_grad = jnp.take(weighted_pad, slot_pair, axis=0).reshape(sp_count, capacity, columns)
    send_in, send_grad = (send_in, send_grad)
    recv_in, recv_grad = (
        lax.all_to_all(send_in, "sp", split_axis=0, concat_axis=0, tiled=True),
        lax.all_to_all(send_grad, "sp", split_axis=0, concat_axis=0, tiled=True),
    )
    rows_in, rows_grad = (
        lax.all_gather(recv_in.reshape(row_total, -1), "tp", axis=1, tiled=True),
        lax.all_gather(recv_grad.reshape(row_total, -1), "tp", axis=1, tiled=True),
    )
    gate_weight = w_gate[0]
    up_weight = w_up[0]
    down_weight = w_down[0]
    gate_pre = jnp.dot(rows_in, gate_weight, preferred_element_type=jnp.float32)
    up_pre = jnp.dot(rows_in, up_weight, preferred_element_type=jnp.float32)
    sigmoid_gate = jax.nn.sigmoid(gate_pre)
    activated = gate_pre * sigmoid_gate
    hidden = (activated * up_pre).astype(jnp.bfloat16)
    hidden_grad = lax.dot_general(
        rows_grad, down_weight, (((1,), (1,)), ((), ())), preferred_element_type=jnp.float32
    )
    down_part = lax.dot_general(
        hidden, rows_grad, (((0,), (0,)), ((), ())), preferred_element_type=jnp.float32
    ).astype(jnp.bfloat16)
    gate_grad = (
        hidden_grad * up_pre * sigmoid_gate * (1.0 + gate_pre * (1.0 - sigmoid_gate))
    ).astype(jnp.bfloat16)
    up_grad = (hidden_grad * activated).astype(jnp.bfloat16)
    gate_part = lax.dot_general(
        rows_in, gate_grad, (((0,), (0,)), ((), ())), preferred_element_type=jnp.float32
    ).astype(jnp.bfloat16)
    up_part = lax.dot_general(
        rows_in, up_grad, (((0,), (0,)), ((), ())), preferred_element_type=jnp.float32
    ).astype(jnp.bfloat16)
    partial_value = lax.dot_general(
        gate_grad, gate_weight, (((1,), (1,)), ((), ())), preferred_element_type=jnp.float32
    )
    partial_value = partial_value + lax.dot_general(
        up_grad, up_weight, (((1,), (1,)), ((), ())), preferred_element_type=jnp.float32
    )
    row_part = lax.psum_scatter(
        partial_value.astype(jnp.bfloat16), "tp", scatter_dimension=1, tiled=True
    )
    back_rows = lax.all_to_all(
        row_part.reshape(sp_count, capacity, -1), "sp", split_axis=0, concat_axis=0, tiled=True
    ).reshape(row_total, -1)
    routed = jnp.sum(
        jnp.take(back_rows, pair_slot, axis=0).astype(jnp.float32).reshape(token_count, TOP, -1),
        axis=1,
    )
    residual_grad = (out_grad.astype(jnp.float32) + routed).astype(jnp.bfloat16)
    full_grad = lax.all_gather(residual_grad, "tp", axis=1, tiled=True)
    grad_proj = lax.psum_scatter(
        lax.dot_general(
            full_grad, mixer_out, (((0,), (0,)), ((), ())), preferred_element_type=jnp.float32
        ).astype(jnp.bfloat16),
        "sp",
        scatter_dimension=0,
        tiled=True,
    ).astype(jnp.float32)
    mixer_grad = jnp.dot(full_grad, w_out, preferred_element_type=jnp.float32)
    query_grad, key_grad, value_grad, decay_grad, state_grad = pull_mixer(mixer_grad)
    state_out_grad = carried_in(
        (log_total, state_grad),
        "sp",
        chain_step,
        (jnp.zeros_like(log_total), jnp.zeros_like(state_grad)),
        True,
    )[1]
    total_grad = jnp.exp(log_total) * jnp.sum(state_out_grad * state_in, axis=2)
    key_extra, value_extra, decay_extra = pull_carry((total_grad, state_out_grad))
    return (
        gate_part[None],
        up_part[None],
        down_part[None],
        grad_proj,
        query_grad.astype(jnp.bfloat16),
        (key_grad + key_extra).astype(jnp.bfloat16),
        (value_grad + value_extra).astype(jnp.bfloat16),
        decay_grad + decay_extra,
    )


def solution(mesh):
    in_specs = (
        P("sp", "tp"),
        P("sp", "tp"),
        P("sp", None),
        P("sp", None),
        P("sp", None, "tp"),
        P("sp", None, "tp"),
        P("sp", "tp", None),
        P(None, "tp"),
        P("sp", "tp"),
        P("sp", "tp"),
        P("sp", "tp"),
        P("sp", "tp"),
    )
    out_specs = (
        P("sp", None, "tp"),
        P("sp", None, "tp"),
        P("sp", "tp", None),
        P("sp", "tp"),
        P("sp", "tp"),
        P("sp", "tp"),
        P("sp", "tp"),
        P("sp", "tp"),
    )
    return jax.shard_map(body, mesh=mesh, in_specs=in_specs, out_specs=out_specs, check_vma=False)
```

profile of v0, /device:TPU:0, one launch (start us, length us, event | category | flops | bytes accessed | tf_op | source)
XLA Modules:
  0.0 410.4 jit_solution(14217362036748022045)
XLA Ops:
  9.5 1.1 reduce-window.6
  11.5 2.4 scatter_custom_fusion
  15.1 2.8 gather_fusion
  18.1 24.4 %all_to_all.15 = bf16[8,80,512]{2,1,0:T(8,128)(2,1)} all-to-all(bf16[8,80,512]{2,1,0:T(8,128)(2,1)S(1)} %broadcast_select_fusion.2), channel_id=1, replica_groups=mesh['sp'=8,'tp'=4] {'sp'}, dimensions={0} | all-to-all | bytes 1310720 | tf_op jit(solution)/shard_map/all_to_all | solution.py:136
  42.8 1.7 mul.251
  44.8 1.4 multiply_convert_fusion.3
  46.3 2.8 gather_fusion.1
  49.3 21.2 %all_to_all.16 = bf16[8,80,512]{2,1,0:T(8,128)(2,1)} all-to-all(bf16[8,80,512]{2,1,0:T(8,128)(2,1)S(1)} %broadcast_select_fusion.1), channel_id=1, replica_groups=mesh['sp'=8,'tp'=4] {'sp'}, dimensions={0} | all-to-all | bytes 1310720 | tf_op jit(solution)/shard_map/all_to_all | solution.py:137
  71.1 9.8 %all-gather.7.cloned.1.call-done = bf16[640,2048]{1,0:T(8,128)(2,1)} async-done(((bf16[640,512]{1,0:T(8,128)(2,1)}), bf16[640,2048]{1,0:T(8,128)(2,1)}) %all-gather.7.cloned.1.call-update) | async-done | bytes 2621456 | tf_op jit(solution)/shard_map/all_gather | solution.py:140
  81.0 3.4 fusion.11
  84.4 2.6 fusion.14
  87.0 35.2 %all-gather.9.cloned.1.call-done = bf16[640,2048]{1,0:T(8,128)(2,1)} async-done(((bf16[640,512]{1,0:T(8,128)(2,1)}), bf16[640,2048]{1,0:T(8,128)(2,1)}) %all-gather.9.cloned.1.call-update) | async-done | bytes 2621456 | tf_op jit(solution)/shard_map/all_gather | solution.py:141
  122.2 4.6 %multiply_convert_fusion.1 = (bf16[640,512]{1,0:T(8,128)(2,1)S(1)}, bf16[640,512]{1,0:T(8,128)(2,1)S(1)}) fusion(f32[640,512]{1,0:T(8,128)S(1)} %fusion.11, f32[640,512]{1,0:T(8,128)} %fusion.14, bf16[640,2048]{1,0:T(8,128)(2,1)} %all-gather.9.cloned.1.call-done, bf16[1,512,2048]{2,1,0:T(8,128)(2,1)} %param.26), kind=kOutput, calls=%fused_computation.48 | convolution fusion | flops 1346437120 | bytes 8650752 | tf_op jit(solution)/shard_map/dot_general | solution.py:151
  126.9 1.6 fusion.9
  128.9 3.1 add_convert_fusion
  133.6 25.9 %fusion.66 = f32[4,64,8,32]{3,2,1,0:T(8,128)S(1)} fusion(f32[4,64,8,32]{3,2,1,0:T(8,128)S(1)} %reshape.284), kind=kOutput, calls=%fused_computation.146 | output fusion | flops 4128768 | bytes 524288 | tf_op jit(solution)/shard_map/jvp(jit(cumsum))/reduce_window_sum | solution.py:40
  162.7 14.1 %all-gather = f32[64,32]{1,0:T(8,128)S(1)} all-gather(f32[8,32]{1,0:T(8,128)S(1)} %get-tuple-element.558), channel_id=2, replica_groups=mesh['sp'=8,'tp'=4] {'sp'}, dimensions={0}, use_global_device_ids=true | all-gather | bytes 9216 | tf_op jit(solution)/shard_map/all_gather | solution.py:17
  178.4 2.0 fusion.38
  180.5 16.9 %all-gather.1 = f32[64,32,64]{2,1,0:T(8,128)S(1)} all-gather(f32[8,32,64]{2,1,0:T(8,128)S(1)} %bitcast.213), channel_id=3, replica_groups=mesh['sp'=8,'tp'=4] {'sp'}, dimensions={0}, use_global_device_ids=true | all-gather | bytes 589824 | tf_op jit(solution)/shard_map/all_gather | solution.py:17
  197.3 1.2 while.64
  199.2 5.0 %all-to-all-start.2 = ((bf16[8,80,512]{2,1,0:T(8,128)(2,1)}), bf16[8,80,512]{2,1,0:T(8,128)(2,1)S(1)}, u32[]{:S(2)}, u32[]{:S(2)}) async-start(bf16[8,80,512]{2,1,0:T(8,128)(2,1)} %bitcast.208), calls=%async_computation.3 | async-start | bytes 1310720 | tf_op jit(solution)/shard_map/all_to_all | solution.py:176
  204.6 6.7 %while.63 = (s32[]{:T(128)}, f32[8,32,64]{2,1,0:T(8,128)S(1)}, f32[4,8,32,64]{3,2,1,0:T(8,128)S(1)}, f32[4,8,32]{2,1,0:T(8,128)S(1)}, f32[4,8,32,1]{2,1,3,0:T(8,...) while((s32[]{:T(128)}, f32[8,32,64]{2,1,0:T(8,128)S(1)}, ...), condition=%wide.region_12.13_spmd, body=%wide.region_11.12_spmd.sunk | while | flops 32770 | bytes 477293 | solution.py:53
  212.1 1.4 rev.6
  213.5 1.6 copy.117
  215.1 1.3 compare_and_fusion
  216.3 1.4 copy.118
  217.8 1.3 pad_clamp_fusion
  219.7 1.9 convolution_multiply_fusion.1
  222.6 1.6 convolution_bitcast_fusion.1
  224.3 2.1 gather_fusion.2
  226.6 2.4 convert_reduce_fusion
  229.0 1.7 add_convert_fusion.1
  230.8 3.1 fusion.20
  234.6 5.0 %fusion.6 = bf16[1,2048,512]{2,1,0:T(8,128)(2,1)} fusion(bf16[640,2048]{1,0:T(8,128)(2,1)} %all-gather.7.cloned.1.call-done, bf16[640,512]{1,0:T(8,128)(2,1)S(1)} %copy-done.28), kind=kOutput, calls=%fused_computation.28 | convolution fusion | flops 1343225856 | bytes 5373952 | tf_op jit(solution)/shard_map/dot_general | solution.py:161
  239.7 3.2 fusion.7
  242.9 3.3 fusion.8
  246.2 11.6 %all-gather.11.cloned.1.call-done = bf16[256,2048]{1,0:T(8,128)(2,1)} async-done(((bf16[256,512]{1,0:T(8,128)(2,1)}), bf16[256,2048]{1,0:T(8,128)(2,1)}) %all-gather.11.cloned.1.call-update) | async-done | bytes 1048592 | tf_op jit(solution)/shard_map/all_gather | solution.py:184
  257.7 3.3 convolution_convert_fusion
  261.0 1.2 copy-done.17
  262.2 2.3 fusion.69
  264.5 1.2 reshape.240
  265.7 1.6 copy.133
  267.3 2.5 fusion.27
  270.8 12.7 %while.65 = (s32[]{:T(128)}, f32[8,32,64]{2,1,0:T(8,128)S(1)}, f32[4,8,32]{2,1,0:T(8,128)S(1)}, f32[4,8,32,64]{3,2,1,0:T(8,128)}, f32[4,8,32,64]{3,2,1,0:T(8,128...) while((s32[]{:T(128)}, f32[8,32,64]{2,1,0:T(8,128)S(1)}, ...), condition=%wide.region_16.17_spmd.clone, body=%wide.region_14.16_spmd.clone.sunk | while | flops 98308 | bytes 472220 | solution.py:53
  272.1 1.1 fusion.113
  275.3 1.1 fusion.113
  281.6 1.1 fusion.113
  283.5 2.8 fusion.41
  286.3 19.8 %all-gather.2 = f32[64,32,64]{2,1,0:T(8,128)} all-gather(f32[8,32,64]{2,1,0:T(8,128)S(1)} %get-tuple-element.402), channel_id=4, replica_groups=mesh['sp'=8,'tp'=4] {'sp'}, dimensions={0}, use_global_device_ids=true | all-gather | bytes 589824 | tf_op jit(solution)/shard_map/all_gather | solution.py:17
  306.0 2.3 rev.7
  308.3 12.5 %while.66 = (s32[]{:T(128)}, f32[8,32,64]{2,1,0:T(8,128)S(1)}, s32[]{:T(128)}, f32[8,8,32]{2,1,0:T(8,128)}, f32[8,8,32,64]{3,2,1,0:T(8,128)}, /*index=5*/s32[]{:T(128)}, s32[]{:T(128)}) while((s32[]{:T(128)}, f32[8,32,64]{2,1,0:T(8,128)S(1)}, s32[]{:T(128)}, f32[8,8,32]{2,1,0:T(8,128)}, f32[8,8,32,64]{3,2,1,0:T(8,128)}, ...), condition=%wide.region_18.19_spmd.clone, body=%wide.region_17.18_spmd.clone.sunk | while | flops 65540 | bytes 199793 | solution.py:29
  322.9 2.1 fusion.30
  327.1 2.9 pad_add_fusion.1
  330.9 1.3 convert_element_type.101
  332.9 1.9 copy.139
  334.8 1.2 convert_element_type.103
  336.7 1.9 fusion.70
  338.7 1.2 convolution_add_fusion.1
  339.9 2.0 fusion.22
  344.2 2.0 fusion.36
  347.6 1.4 copy.149
  349.0 25.7 %fusion.67 = f32[4,64,8,32]{3,2,1,0:T(8,128)S(1)} fusion(f32[4,64,8,32]{3,2,1,0:T(8,128)S(1)} %copy.145), kind=kOutput, calls=%fused_computation.147 | output fusion | flops 4128768 | bytes 524288 | tf_op jit(solution)/shard_map/transpose(jvp(jit(cumsum)))/reduce_window_sum | solution.py:40
  374.7 25.8 %fusion.68 = f32[4,64,8,32]{3,2,1,0:T(8,128)S(1)} fusion(f32[4,64,8,32]{3,2,1,0:T(8,128)S(1)} %copy-done.16), kind=kOutput, calls=%fused_computation.148 | output fusion | flops 4128768 | bytes 524288 | tf_op jit(solution)/shard_map/transpose(jvp(jit(cumsum)))/reduce_window_sum | solution.py:64
  401.6 1.8 convert_element_type.99
  (249 shorter events, 58.1 us)
Async XLA Ops:
  7.2 73.8 %copy-start = (bf16[1,2048,512]{2,1,0:T(8,128)(2,1)S(1)}, bf16[1,2048,512]{2,1,0:T(8,128)(2,1)}, u32[]{:S(2)}) copy-start(bf16[1,2048,512]{2,1,0:T(8,128)(2,1)} %param.24) | copy-start | bytes 6291460
  7.2 73.8 %all-gather.7.cloned.1.call-start = ((), (), s32[]{:S(2)}) async-start(), calls=%async_computation.5 | async-start | bytes 3276800 | tf_op jit(solution)/shard_map/all_gather | solution.py:140
  11.0 0.6 copy-start.43
  11.0 3.0 copy-start.45
  17.9 24.6 %copy-start.26 = (bf16[256,512]{1,0:T(8,128)(2,1)S(1)}, bf16[256,512]{1,0:T(8,128)(2,1)}, u32[]{:S(2)}) copy-start(bf16[256,512]{1,0:T(8,128)(2,1)} %param.21) | copy-start | bytes 786436
  42.5 2.1 copy-start.46
  42.5 79.7 %all-gather.9.cloned.1.call-start = ((), (), s32[]{:S(2)}) async-start(), calls=%async_computation.6 | async-start | bytes 3276800 | tf_op jit(solution)/shard_map/all_gather | solution.py:141
  70.6 128.7 %reduce-scatter.3.cloned.1.call-start = ((), (), s32[]{:S(2)}) async-start(), calls=%async_computation.7 | async-start | bytes 3276800 | tf_op jit(solution)/shard_map/reduce_scatter | solution.py:173
  81.0 3.4 copy-start.20
  81.0 3.4 copy-start.47
  84.4 37.8 %copy-start.50 = (f32[640,512]{1,0:T(8,128)}, f32[640,512]{1,0:T(8,128)S(1)}, u32[]{:S(2)}) copy-start(f32[640,512]{1,0:T(8,128)S(1)} %fusion.11) | copy-start | bytes 3932164
  126.9 1.6 copy-start.27
  126.9 1.6 copy-start.29
  126.9 2.1 copy-start.21
  132.0 0.9 copy-start.38
  132.0 1.3 copy-start.35
  133.6 26.3 %copy-start.39 = (bf16[256,256]{1,0:T(8,128)(2,1)S(1)}, bf16[256,256]{1,0:T(8,128)(2,1)}, u32[]{:S(2)}) copy-start(bf16[256,256]{1,0:T(8,128)(2,1)} %param.28) | copy-start | bytes 393220
  159.5 1.0 copy-start.15
  159.5 1.2 copy-start.36
  159.9 59.2 %copy-start.2 = (f32[4,64,8,32]{1,3,2,0:T(8,128)}, f32[4,64,8,32]{1,3,2,0:T(8,128)S(1)}, u32[]{:S(2)}) copy-start(f32[4,64,8,32]{1,3,2,0:T(8,128)S(1)} %copy.122) | copy-start | bytes 786436
  160.7 17.6 %copy-start.12 = (f32[4,64,8,32]{1,0,3,2:T(4,128)}, f32[4,64,8,32]{1,0,3,2:T(4,128)S(1)}, u32[]{:S(2)}) copy-start(f32[4,64,8,32]{1,0,3,2:T(4,128)S(1)} %reshape.242) | copy-start | bytes 786436
  161.8 16.6 %copy-start.41 = (f32[8,32]{1,0:T(8,128)}, f32[8,32]{1,0:T(8,128)S(1)}, u32[]{:S(2)}) copy-start(f32[8,32]{1,0:T(8,128)S(1)} %get-tuple-element.558) | copy-start | bytes 3076
  162.5 15.8 %copy-start.31 = (f32[4,8,32]{2,1,0:T(8,128)}, f32[4,8,32]{2,1,0:T(8,128)S(1)}, u32[]{:S(2)}) copy-start(f32[4,8,32]{2,1,0:T(8,128)S(1)} %fusion.25) | copy-start | bytes 12292
  177.0 0.8 copy-start.8
  178.4 2.1 copy-start.18
  198.6 0.6 copy-start.37
  199.2 5.1 %copy-start.10 = (f32[8,32,64]{2,1,0:T(8,128)}, f32[8,32,64]{2,1,0:T(8,128)S(1)}, u32[]{:S(2)}) copy-start(f32[8,32,64]{2,1,0:T(8,128)S(1)} %get-tuple-element.750) | copy-start | bytes 196612
  199.2 25.0 %all-to-all-start.2 = ((bf16[8,80,512]{2,1,0:T(8,128)(2,1)}), bf16[8,80,512]{2,1,0:T(8,128)(2,1)S(1)}, u32[]{:S(2)}, u32[]{:S(2)}) async-start(bf16[8,80,512]{2,1,0:T(8,128)(2,1)} %bitcast.208), calls=%async_computation.3 | async-start | bytes 1310720 | tf_op jit(solution)/shard_map/all_to_all | solution.py:176
  204.3 7.0 %copy-start.44 = (s32[512]{0:T(512)S(1)}, s32[512]{0:T(512)}, u32[]{:S(2)}) copy-start(s32[512]{0:T(512)} %copy-done.43) | copy-start | bytes 6148
  204.3 53.4 %all-gather.11.cloned.1.call-start = ((), (), s32[]{:S(2)}) async-start(), calls=%async_computation.8 | async-start | bytes 1310720 | tf_op jit(solution)/shard_map/all_gather | solution.py:184
  211.3 0.8 copy-start.40
  211.3 19.5 %copy-start.4 = (f32[4,8,32,64]{3,2,1,0:T(8,128)}, f32[4,8,32,64]{3,2,1,0:T(8,128)S(1)}, u32[]{:S(2)}) copy-start(f32[4,8,32,64]{3,2,1,0:T(8,128)S(1)} %get-tuple-element.779) | copy-start | bytes 786436
  219.1 0.6 copy-start.33
  221.6 1.0 copy-start.6
  230.7 170.9 %reduce-scatter.5.cloned.1.call-start = ((), (), s32[]{:S(2)}) async-start(), calls=%async_computation.9 | async-start | bytes 2359296 | tf_op jit(solution)/shard_map/reduce_scatter | solution.py:185
  230.8 3.8 copy-start.28
  234.6 5.1 %copy-start.30 = (bf16[640,512]{1,0:T(8,128)(2,1)S(1)}, bf16[640,512]{1,0:T(8,128)(2,1)}, u32[]{:S(2)}) copy-start(bf16[640,512]{1,0:T(8,128)(2,1)} %copy-done.29) | copy-start | bytes 1966084
  234.6 5.1 %copy-start.48 = (bf16[640,2048]{1,0:T(8,128)(2,1)S(1)}, bf16[640,2048]{1,0:T(8,128)(2,1)}, u32[]{:S(2)}) copy-start(bf16[640,2048]{1,0:T(8,128)(2,1)} %all-gather.7.cloned.1.call-done) | copy-start | bytes 7864324
  239.7 3.2 copy-start.49
  239.7 3.2 copy-start.51
  239.7 3.2 copy-start.52
  261.0 1.2 copy-start.17
  270.8 12.7 %copy-start.3 = (f32[4,64,8,32]{1,3,2,0:T(8,128)S(1)}, f32[4,64,8,32]{1,3,2,0:T(8,128)}, u32[]{:S(2)}) copy-start(f32[4,64,8,32]{1,3,2,0:T(8,128)} %copy-done.2) | copy-start | bytes 786436
  306.0 15.8 %copy-start.32 = (f32[4,8,32]{2,1,0:T(8,128)S(1)}, f32[4,8,32]{2,1,0:T(8,128)}, u32[]{:S(2)}) copy-start(f32[4,8,32]{2,1,0:T(8,128)} %copy-done.31) | copy-start | bytes 12292
  320.8 4.2 %copy-start.34 = (f32[64,64]{1,0:T(8,128)S(1)}, f32[64,64]{1,0:T(8,128)}, u32[]{:S(2)}) copy-start(f32[64,64]{1,0:T(8,128)} %copy-done.33) | copy-start | bytes 49156
  321.9 3.1 copy-start.5
  325.0 2.1 copy-start.13
  325.0 2.1 copy-start.24
  325.0 2.1 copy-start.25
  330.0 6.8 %copy-start.9 = (f32[4,64,8,32]{1,3,2,0:T(8,128)S(1)}, f32[4,64,8,32]{1,3,2,0:T(8,128)}, u32[]{:S(2)}) copy-start(f32[4,64,8,32]{1,3,2,0:T(8,128)} %copy-done.8) | copy-start | bytes 786436
  330.0 6.8 %copy-start.14 = (f32[4,8,32,64]{3,2,1,0:T(8,128)S(1)}, f32[4,8,32,64]{3,2,1,0:T(8,128)}, u32[]{:S(2)}) copy-start(f32[4,8,32,64]{3,2,1,0:T(8,128)} %get-tuple-element.401) | copy-start | bytes 786436
  330.9 7.8 %copy-start.7 = (f32[4,8,64,64]{3,2,1,0:T(8,128)S(1)}, f32[4,8,64,64]{3,2,1,0:T(8,128)}, u32[]{:S(2)}) copy-start(f32[4,8,64,64]{3,2,1,0:T(8,128)} %copy-done.6) | copy-start | bytes 1572868
  339.9 3.6 copy-start.23
  341.9 2.3 copy-start.19
  343.5 3.1 copy-start.11
  343.5 3.3 copy-start.42
  343.9 3.5 copy-start.22
  349.0 25.7 %copy-start.16 = (f32[4,64,8,32]{3,2,1,0:T(8,128)S(1)}, f32[4,64,8,32]{3,2,1,0:T(8,128)}, u32[]{:S(2)}) copy-start(f32[4,64,8,32]{3,2,1,0:T(8,128)} %copy.149) | copy-start | bytes 786436
  374.7 28.7 %copy-start.1 = (bf16[1,2048,512]{2,1,0:T(8,128)(2,1)S(1)}, bf16[1,2048,512]{2,1,0:T(8,128)(2,1)}, u32[]{:S(2)}) copy-start(bf16[1,2048,512]{2,1,0:T(8,128)(2,1)} %param.24) | copy-start | bytes 6291460
Sparse Core Ops, SparseCore 0:
  42.6 38.3 all-gather.6
  82.8 39.3 all-gather.8
  132.2 39.5 reduce-scatter.2
  230.8 26.8 all-gather.10
  261.2 36.9 reduce-scatter.4
where the time goes:
time: 417 us; the launch traced here: 410 us
  other arithmetic  115 us (28%)
  blocking collectives  96.4 us (23%)
  matrix products  62.1 us (15%)
  local copies, waits for them, and re-layouts  58.6 us (14%)
  waiting for transfers between devices  56.7 us (14%)
  between operations  15.2 us (4%)
  starting transfers between devices  5.94 us (1%)
    another operation x2, other arithmetic, mixer_pass(): cumulative = jnp.cumsum(decays, axis=1)  51.5 us
    all_gather x3, blocking collectives, carried_in(): pieces = jax.tree.map(lambda part: lax.all_gather(part, axis), value)  50.8 us
    all_gather x1, waiting for transfers between devices, body(): lax.all_gather(recv_grad.reshape(row_total, -1), 'tp', axis=1, tiled=True)  35.2 us
    another operation x1, other arithmetic, carry_terms(): jnp.cumsum(decay_full.reshape(blocks, BLOCK, nheads, KEY_CHANNELS), axis=1)  25.8 us
    all_to_all x1, blocking collectives, body(): lax.all_to_all(send_in, 'sp', split_axis=0, concat_axis=0, tiled=True)  24.4 us
    all_to_all x1, blocking collectives, body(): lax.all_to_all(send_grad, 'sp', split_axis=0, concat_axis=0, tiled=True)  21.2 us
    all_gather x1, waiting for transfers between devices, body(): full_grad = lax.all_gather(residual_grad, 'tp', axis=1, tiled=True)  11.6 us
    all_gather x1, waiting for transfers between devices, body(): lax.all_gather(recv_in.reshape(row_total, -1), 'tp', axis=1, tiled=True)  9.84 us
  transfers between devices with their start and end apart: 6, of which 3 were waited for; matrix products, arithmetic and copies ran while one was open for 48% of the time, Pallas kernels for 0%

commit v1 on v0

--- a/solution.py
+++ b/solution.py
@@ -12,21 +12,32 @@
 PRECISE = lax.Precision.HIGHEST
 
 
-def carried_in(value, axis, join, neutral, backward):
-    count, mine = (lax.axis_size(axis), lax.axis_index(axis))
-    pieces = jax.tree.map(lambda part: lax.all_gather(part, axis), value)
+def gathered_spans(log_total, increment):
+    rows, width = log_total.size, increment.shape[-1]
+    packed = jnp.concatenate([increment.reshape(rows, width), log_total.reshape(-1, width)], axis=0)
+    spans = lax.all_gather(packed, "sp")
+    return (spans[:, rows:].reshape(-1, rows), spans[:, :rows])
+
+
+def carried_in(span_logs, span_states, backward):
+    count, mine = (lax.axis_size("sp"), lax.axis_index("sp"))
+    source = jnp.arange(count)
     if backward:
-        pieces = jax.tree.map(lambda part: part[::-1], pieces)
-        mine = count - 1 - mine
-    subtotal = jax.tree.map(
-        lambda part, zero: jnp.full_like(part, 0) + jnp.asarray(zero, part.dtype), value, neutral
-    )
-
-    def hop(position, subtotal):
-        longer = join(subtotal, jax.tree.map(lambda part: part[position], pieces))
-        return jax.tree.map(lambda new, old: jnp.where(position < mine, new, old), longer, subtotal)
-
-    return lax.fori_loop(0, count - 1, hop, subtotal)
+        between = (source[None, :] < source[:, None]) & (source[None, :] > mine)
+        counts = source > mine
+    else:
+        between = (source[None, :] > source[:, None]) & (source[None, :] < mine)
+        counts = source < mine
+    logs = jnp.dot(between.astype(jnp.float32), span_logs, precision=PRECISE)
+    weights = jnp.where(counts[:, None], jnp.exp(logs), 0.0)
+    return jnp.sum(weights[:, :, None] * span_states, axis=0)
+
+
+def running_sum(values, axis):
+    length = values.shape[axis]
+    ones = jnp.tril(jnp.ones((length, length), jnp.float32))
+    moved = jnp.tensordot(ones, values, axes=((1,), (axis,)), precision=PRECISE)
+    return jnp.moveaxis(moved, 0, axis)
 
 
 def mixer_pass(queries, key_rows, value_rows, log_decay, state_in):
@@ -37,7 +48,7 @@
     key_blocks = key_rows.reshape(blocks, BLOCK, nheads, KEY_CHANNELS) * KEY_CHANNELS ** (-0.5)
     value_blocks = value_rows.reshape(blocks, BLOCK, nheads, VAL_DIM)
     decays = log_decay.reshape(blocks, BLOCK, nheads, KEY_CHANNELS)
-    cumulative = jnp.cumsum(decays, axis=1)
+    cumulative = running_sum(decays, 1)
     closing = cumulative[:, -1]
     query_scaled = query_blocks * jnp.exp(cumulative)
     key_scaled = key_blocks * jnp.exp(-cumulative)
@@ -50,7 +61,7 @@
     def advance(state_now, pieces):
         return (jnp.exp(pieces[0])[..., None] * state_now + pieces[1], state_now)
 
-    state_out, entering = lax.scan(advance, state_in, (closing, additions))
+    state_out, entering = lax.scan(advance, state_in, (closing, additions), unroll=True)
     carried = jnp.einsum("nthd,nhdv->nthv", query_scaled, entering, precision=PRECISE)
     return (within + carried).reshape(length, nheads * VAL_DIM)
 
@@ -61,18 +72,14 @@
     nheads = key_full.shape[1] // KEY_CHANNELS
     key_blocks = key_full.reshape(blocks, BLOCK, nheads, KEY_CHANNELS) * KEY_CHANNELS ** (-0.5)
     value_blocks = value_full.reshape(blocks, BLOCK, nheads, VAL_DIM)
-    cumulative = jnp.cumsum(decay_full.reshape(blocks, BLOCK, nheads, KEY_CHANNELS), axis=1)
+    cumulative = running_sum(decay_full.reshape(blocks, BLOCK, nheads, KEY_CHANNELS), 1)
     closing = cumulative[:, -1]
     key_tail = key_blocks * jnp.exp(closing[:, None] - cumulative)
     additions = jnp.einsum("nshd,nshv->nhdv", key_tail, value_blocks, precision=PRECISE)
     log_total = jnp.sum(closing, axis=0)
-    remaining = log_total[None] - jnp.cumsum(closing, axis=0)
+    remaining = log_total[None] - running_sum(closing, 0)
     increment = jnp.einsum("nhd,nhdv->hdv", jnp.exp(remaining), additions, precision=PRECISE)
     return (log_total, increment)
-
-
-def chain_step(earlier, latter):
-    return (earlier[0] + latter[0], jnp.exp(latter[0])[..., None] * earlier[1] + latter[1])
 
 
 def body(
@@ -97,13 +104,8 @@
     key_full = key_rows.astype(jnp.float32)
     value_full = value_rows.astype(jnp.float32)
     (log_total, increment), pull_carry = jax.vjp(carry_terms, key_full, value_full, log_decay)
-    state_in = carried_in(
-        (log_total, increment),
-        "sp",
-        chain_step,
-        (jnp.zeros_like(log_total), jnp.zeros_like(increment)),
-        False,
-    )[1]
+    span_logs, span_states = gathered_spans(log_total, increment)
+    state_in = carried_in(span_logs, span_states, False).reshape(increment.shape)
     mixer_raw, pull_mixer = jax.vjp(
         mixer_pass, query_full, key_full, value_full, log_decay, state_in
     )
@@ -131,7 +133,6 @@
     inputs_pad = jnp.concatenate([moe_input, jnp.zeros((1, columns), jnp.bfloat16)], axis=0)
     send_in = jnp.take(inputs_pad, slot_token, axis=0).reshape(sp_count, capacity, columns)
     send_grad = jnp.take(weighted_pad, slot_pair, axis=0).reshape(sp_count, capacity, columns)
-    send_in, send_grad = (send_in, send_grad)
     recv_in, recv_grad = (
         lax.all_to_all(send_in, "sp", split_axis=0, concat_axis=0, tiled=True),
         lax.all_to_all(send_grad, "sp", split_axis=0, concat_axis=0, tiled=True),
@@ -192,13 +193,8 @@
     ).astype(jnp.float32)
     mixer_grad = jnp.dot(full_grad, w_out, preferred_element_type=jnp.float32)
     query_grad, key_grad, value_grad, decay_grad, state_grad = pull_mixer(mixer_grad)
-    state_out_grad = carried_in(
-        (log_total, state_grad),
-        "sp",
-        chain_step,
-        (jnp.zeros_like(log_total), jnp.zeros_like(state_grad)),
-        True,
-    )[1]
+    span_grads = lax.all_gather(state_grad.reshape(log_total.size, -1), "sp")
+    state_out_grad = carried_in(span_logs, span_grads, True).reshape(increment.shape)
     total_grad = jnp.exp(log_total) * jnp.sum(state_out_grad * state_in, axis=2)
     key_extra, value_extra, decay_extra = pull_carry((total_grad, state_out_grad))
     return (

time: 417 us -> 336 us (0.81)
  other arithmetic: 115 us -> 25.7 us
  blocking collectives: 96.4 us -> 78.7 us
  waiting for transfers between devices: 56.7 us -> 73.3 us
  matrix products: 62.1 us -> 73.5 us
    another operation x7 -> x2, other arithmetic: 79.8 us -> 1.18 us  [the longest x2 51.5 us: mixer_pass(): cumulative = jnp.cumsum(decays, axis=1)]
    all_gather x3 -> x2, blocking collectives: 50.8 us -> 33 us  [the longest x1 17.2 us: body(): span_grads = lax.all_gather(state_grad.reshape(log_total.size, -1), 'sp')]
    reduce_scatter x1, waiting for transfers between devices: 0.02 us -> 12.5 us  [body(): lax.psum_scatter(partial_value.astype(jnp.bfloat16), 'tp', scatter_dimens...]
    all_to_all x1, waiting for transfers between devices: 0.01 us -> 11.3 us  [body(): lax.all_to_all(row_part.reshape(sp_count, capacity, -1), 'sp', split_axis...]
    select_n x15 -> x1, other arithmetic: 8.18 us -> 0.01 us  [running_sum(): ones = jnp.tril(jnp.ones((length, length), jnp.float32))]
    squeeze x0 -> x4, local copies, waits for them, and re-layouts: none -> 6.52 us  [mixer_pass(): lax.scan(advance, state_in, (closing, additions), unroll=True)]
    dynamic_update_slice x8 -> x0, other arithmetic: 5.43 us -> none  [mixer_pass(): state_out, entering = lax.scan(advance, state_in, (closing, additions))]
    all_gather x1, waiting for transfers between devices: 11.6 us -> 6.37 us  [body(): full_grad = lax.all_gather(residual_grad, 'tp', axis=1, tiled=True)]
  transfers between devices with their start and end apart: 6 -> 6, of which waited for: 3 -> 5; matrix products, arithmetic and copies ran while one was open for 48% -> 32% of each run, Pallas kernels for 0% -> 0%
where the time goes in v1:
time: 336 us; the launch traced here: 330 us
  blocking collectives  78.7 us (23%)
  matrix products  73.5 us (22%)
  waiting for transfers between devices  73.3 us (22%)
  local copies, waits for them, and re-layouts  59.2 us (18%)
  other arithmetic  25.7 us (8%)
  between operations  15.1 us (4%)
  starting transfers between devices  4.99 us (1%)
    all_gather x1, waiting for transfers between devices, body(): lax.all_gather(recv_grad.reshape(row_total, -1), 'tp', axis=1, tiled=True)  34.1 us
    all_to_all x1, blocking collectives, body(): lax.all_to_all(send_in, 'sp', split_axis=0, concat_axis=0, tiled=True)  24.4 us
    all_to_all x1, blocking collectives, body(): lax.all_to_all(send_grad, 'sp', split_axis=0, concat_axis=0, tiled=True)  21.2 us
    all_gather x1, blocking collectives, body(): span_grads = lax.all_gather(state_grad.reshape(log_total.size, -1), 'sp')  17.2 us
    all_gather x1, blocking collectives, gathered_spans(): spans = lax.all_gather(packed, 'sp')  15.9 us
    reduce_scatter x1, waiting for transfers between devices, body(): lax.psum_scatter(partial_value.astype(jnp.bfloat16), 'tp', scatter_dimens...  12.5 us
    all_to_all x1, waiting for transfers between devices, body(): lax.all_to_all(row_part.reshape(sp_count, capacity, -1), 'sp', split_axis...  11.3 us
    unnamed x139, local copies, waits for them, and re-layouts  9.08 us
  transfers between devices with their start and end apart: 6, of which 5 were waited for; matrix products, arithmetic and copies ran while one was open for 32% of the time, Pallas kernels for 0%

profile of v1, /device:TPU:0, one launch (start us, length us, event | category | flops | bytes accessed | tf_op | source)
XLA Modules:
  0.0 330.4 jit_solution(16253422859487722867)
XLA Ops:
  9.5 1.1 reduce-window.6
  11.0 2.4 scatter_custom_fusion
  14.6 2.8 gather_fusion
  17.5 24.4 %all_to_all.15 = bf16[8,80,512]{2,1,0:T(8,128)(2,1)} all-to-all(bf16[8,80,512]{2,1,0:T(8,128)(2,1)S(1)} %broadcast_select_fusion.2), channel_id=1, replica_groups=mesh['sp'=8,'tp'=4] {'sp'}, dimensions={0} | all-to-all | bytes 1310720 | tf_op jit(solution)/shard_map/all_to_all | solution.py:137
  42.3 1.7 mul.335
  44.3 1.4 multiply_convert_fusion.3
  46.4 2.8 gather_fusion.1
  50.0 21.2 %all_to_all.16 = bf16[8,80,512]{2,1,0:T(8,128)(2,1)} all-to-all(bf16[8,80,512]{2,1,0:T(8,128)(2,1)S(1)} %broadcast_select_fusion.1), channel_id=1, replica_groups=mesh['sp'=8,'tp'=4] {'sp'}, dimensions={0} | all-to-all | bytes 1310720 | tf_op jit(solution)/shard_map/all_to_all | solution.py:138
  71.5 9.0 %all-gather.6.cloned.1.call-done = bf16[640,2048]{1,0:T(8,128)(2,1)} async-done(((bf16[640,512]{1,0:T(8,128)(2,1)}), bf16[640,2048]{1,0:T(8,128)(2,1)}) %all-gather.6.cloned.1.call-update) | async-done | bytes 2621456 | tf_op jit(solution)/shard_map/all_gather | solution.py:141
  80.4 4.5 %fusion.5 = f32[640,512]{1,0:T(8,128)} fusion(bf16[640,2048]{1,0:T(8,128)(2,1)} %all-gather.6.cloned.1.call-done, bf16[1,2048,512]{2,1,0:T(8,128)(2,1)S(1)} %copy-done), kind=kOutput, calls=%fused_computation.14 | convolution fusion | flops 1342177280 | bytes 6029312 | tf_op jit(solution)/shard_map/dot_general | solution.py:147
  84.9 2.7 fusion.8
  87.6 34.1 %all-gather.8.cloned.1.call-done = bf16[640,2048]{1,0:T(8,128)(2,1)} async-done(((bf16[640,512]{1,0:T(8,128)(2,1)}), bf16[640,2048]{1,0:T(8,128)(2,1)}) %all-gather.8.cloned.1.call-update) | async-done | bytes 2621456 | tf_op jit(solution)/shard_map/all_gather | solution.py:142
  121.7 5.1 %multiply_convert_fusion.1 = (bf16[640,512]{1,0:T(8,128)(2,1)S(1)}, bf16[640,512]{1,0:T(8,128)(2,1)S(1)}) fusion(f32[640,512]{1,0:T(8,128)} %fusion.5, f32[640,512]{1,0:T(8,128)} %fusion.8, bf16[640,2048]{1,0:T(8,128)(2,1)} %all-gather.8.cloned.1.call-done, bf16[1,512,2048]{2,1,0:T(8,128)(2,1)} %param.18), kind=kOutput, calls=%fused_computation.29 | convolution fusion | flops 1346437120 | bytes 8650752 | tf_op jit(solution)/shard_map/dot_general | solution.py:152
  126.8 1.6 fusion.3
  128.9 3.0 add_convert_fusion
  138.1 1.4 fusion.64
  139.4 3.1 fusion.55
  142.7 15.9 %all-gather.1 = f32[8,260,64]{1,2,0:T(8,128)S(1)} all-gather(f32[1,260,64]{1,2,0:T(8,128)S(1)} %copy.359), channel_id=2, replica_groups=mesh['sp'=8,'tp'=4] {'sp'}, dimensions={0}, use_global_device_ids=true | all-gather | bytes 599040 | tf_op jit(solution)/shard_map/all_gather | solution.py:18
  159.1 12.5 %reduce-scatter.3.cloned.1.call-done = bf16[640,512]{1,0:T(8,128)(2,1)} async-done(((bf16[640,2048]{1,0:T(8,128)(2,1)}), bf16[640,512]{1,0:T(8,128)(2,1)}) %reduce-scatter.3.cloned.1.call-update) | async-done | bytes 655376 | tf_op jit(solution)/shard_map/reduce_scatter | solution.py:174
  171.6 4.6 %all-to-all-start.2 = ((bf16[8,80,512]{2,1,0:T(8,128)(2,1)}), bf16[8,80,512]{2,1,0:T(8,128)(2,1)S(1)}, u32[]{:S(2)}, u32[]{:S(2)}) async-start(bf16[8,80,512]{2,1,0:T(8,128)(2,1)} %bitcast.234), calls=%async_computation.3 | async-start | bytes 1310720 | tf_op jit(solution)/shard_map/all_to_all | solution.py:177
  176.8 1.7 bitcast_add_fusion.1
  178.5 1.9 convolution_multiply_fusion.1
  181.4 1.6 convolution_bitcast_fusion.1
  183.1 11.3 %all-to-all-done.2 = bf16[8,80,512]{2,1,0:T(8,128)(2,1)S(1)} async-done(((bf16[8,80,512]{2,1,0:T(8,128)(2,1)}), bf16[8,80,512]{2,1,0:T(8,128)(2,1)S(1)}, u32[]{:S(2)}, u32[]{:S(2)}) %all-to-all-start.2) | async-done | bytes 655392 | tf_op jit(solution)/shard_map/all_to_all | solution.py:177
  194.4 2.0 gather_fusion.2
  196.6 1.7 convert_reduce_fusion
  203.8 1.8 multiply_add_fusion.3
  205.5 5.2 %fusion = bf16[1,2048,512]{2,1,0:T(8,128)(2,1)} fusion(bf16[640,2048]{1,0:T(8,128)(2,1)} %all-gather.6.cloned.1.call-done, bf16[640,512]{1,0:T(8,128)(2,1)} %copy-done.25), kind=kOutput, calls=%fused_computation.9 | convolution fusion | flops 1343225856 | bytes 5373952 | tf_op jit(solution)/shard_map/dot_general | solution.py:162
  210.7 3.2 fusion.1
  213.9 3.3 fusion.2
  217.2 6.4 %all-gather.10.cloned.1.call-done = bf16[256,2048]{1,0:T(8,128)(2,1)} async-done(((bf16[256,512]{1,0:T(8,128)(2,1)}), bf16[256,2048]{1,0:T(8,128)(2,1)}) %all-gather.10.cloned.1.call-update) | async-done | bytes 1048592 | tf_op jit(solution)/shard_map/all_gather | solution.py:185
  223.6 2.6 fusion.140
  226.2 1.2 reshape.505
  227.4 1.6 copy.364
  229.0 2.5 fusion.25
  231.5 2.6 multiply_reduce_fusion.2
  234.2 1.9 fusion.28
  236.1 1.8 fusion.14
  237.9 1.1 copy.363
  239.0 2.1 convert_element_type.99
  241.1 3.5 %convolution_convert_fusion = bf16[2048,512]{1,0:T(8,128)(2,1)} fusion(bf16[256,2048]{1,0:T(8,128)(2,1)} %all-gather.10.cloned.1.call-done, bf16[256,512]{1,0:T(8,128)(2,1)} %convert_element_type.99), kind=kOutput, calls=%fused_computation.5 | convolution fusion | flops 537919488 | bytes 3407872 | tf_op jit(solution)/shard_map/dot_general | solution.py:187
  244.7 1.9 multiply_add_fusion
  246.6 1.7 copy.372
  248.2 1.6 copy.371
  249.8 1.6 copy.370
  251.5 1.6 copy.369
  254.0 17.2 %all_gather.23 = f32[8,256,64]{1,2,0:T(8,128)S(1)} all-gather(f32[1,256,64]{1,2,0:T(8,128)S(1)} %multiply_add_fusion.5), channel_id=1, replica_groups=mesh['sp'=8,'tp'=4] {'sp'}, dimensions={0}, use_global_device_ids=true | all-gather | bytes 589824 | tf_op jit(solution)/shard_map/all_gather | solution.py:196
  271.2 2.7 convolution_bitcast_fusion.4
  275.5 2.3 convolution_multiply_fusion
  278.9 1.8 fusion.17
  280.8 2.7 multiply_multiply_fusion
  284.4 1.8 convert_element_type.103
  286.2 1.7 copy.392
  287.9 1.9 copy.376
  289.7 1.8 convert_element_type.105
  291.6 1.7 copy.393
  293.2 3.1 fusion.57
  296.4 1.2 convolution_add_fusion.1
  297.7 2.0 fusion.16
  303.2 1.4 fusion.80
  307.8 3.7 %fusion.53 = f32[8,32,1,4]{3,2,1,0:T(1,128)} fusion(f32[8,32,64,1]{2,3,1,0:T(1,128)S(1)} %bitcast.233, f32[4,8,32,64]{3,2,1,0:T(8,128)} %fusion.64), kind=kOutput, calls=%fused_computation.101 | convolution fusion | flops 786432 | bytes 331776 | tf_op jit(solution)/shard_map/transpose(jvp(nhd,nhdv->hdv))/dot_general | solution.py:81
  316.2 1.3 fusion.81
  317.5 1.1 maximum_add_fusion
  321.9 1.8 convert_element_type.101
  (235 shorter events, 39.5 us)
Async XLA Ops:
  7.2 73.3 %copy-start = (bf16[1,2048,512]{2,1,0:T(8,128)(2,1)S(1)}, bf16[1,2048,512]{2,1,0:T(8,128)(2,1)}, u32[]{:S(2)}) copy-start(bf16[1,2048,512]{2,1,0:T(8,128)(2,1)} %param.16) | copy-start | bytes 6291460
  7.2 73.2 %all-gather.6.cloned.1.call-start = ((), (), s32[]{:S(2)}) async-start(), calls=%async_computation.5 | async-start | bytes 3276800 | tf_op jit(solution)/shard_map/all_gather | solution.py:141
  11.0 2.5 copy-start.57
  17.4 24.6 %copy-start.24 = (bf16[256,512]{1,0:T(8,128)(2,1)S(1)}, bf16[256,512]{1,0:T(8,128)(2,1)}, u32[]{:S(2)}) copy-start(bf16[256,512]{1,0:T(8,128)(2,1)} %param.13) | copy-start | bytes 786436
  41.9 2.1 copy-start.60
  42.0 79.7 %all-gather.8.cloned.1.call-start = ((), (), s32[]{:S(2)}) async-start(), calls=%async_computation.6 | async-start | bytes 3276800 | tf_op jit(solution)/shard_map/all_gather | solution.py:142
  71.2 100.4 %reduce-scatter.3.cloned.1.call-start = ((), (), s32[]{:S(2)}) async-start(), calls=%async_computation.7 | async-start | bytes 3276800 | tf_op jit(solution)/shard_map/reduce_scatter | solution.py:174
  80.4 4.5 %copy-start.19 = (bf16[1,2048,512]{2,1,0:T(8,128)(2,1)S(1)}, bf16[1,2048,512]{2,1,0:T(8,128)(2,1)}, u32[]{:S(2)}) copy-start(bf16[1,2048,512]{2,1,0:T(8,128)(2,1)} %param.17) | copy-start | bytes 6291460
  80.4 4.5 %copy-start.61 = (bf16[640,2048]{1,0:T(8,128)(2,1)S(1)}, bf16[640,2048]{1,0:T(8,128)(2,1)}, u32[]{:S(2)}) copy-start(bf16[640,2048]{1,0:T(8,128)(2,1)} %all-gather.6.cloned.1.call-done) | copy-start | bytes 7864324
  126.8 1.6 copy-start.25
  126.8 1.6 copy-start.26
  126.8 2.1 copy-start.20
  131.9 1.5 copy-start.42
  131.9 1.9 copy-start.39
  132.1 2.2 copy-start.43
  134.6 2.6 copy-start.9
  135.9 3.5 %copy-start.33 = (f32[4,8,32]{2,1,0:T(8,128)}, f32[4,8,32]{2,1,0:T(8,128)S(1)}, u32[]{:S(2)}) copy-start(f32[4,8,32]{2,1,0:T(8,128)S(1)} %get-tuple-element.72) | copy-start | bytes 12292
  137.2 41.3 %copy-start.2 = (f32[4,64,8,32]{1,3,2,0:T(8,128)}, f32[4,64,8,32]{1,3,2,0:T(8,128)S(1)}, u32[]{:S(2)}) copy-start(f32[4,64,8,32]{1,3,2,0:T(8,128)S(1)} %get-tuple-element.96) | copy-start | bytes 786436
  139.4 19.7 %copy-start.58 = (s32[512,1]{0,1:T(1,128)S(1)}, s32[512,1]{0,1:T(1,128)}, u32[]{:S(2)}) copy-start(s32[512,1]{0,1:T(1,128)} %copy-done.57) | copy-start | bytes 6148
  159.0 21.5 %copy-start.28 = (f32[256,64]{0,1:T(8,128)}, f32[256,64]{0,1:T(8,128)S(1)}, u32[]{:S(2)}) copy-start(f32[256,64]{0,1:T(8,128)S(1)} %fusion.30) | copy-start | bytes 196612
  171.6 22.7 %all-to-all-start.2 = ((bf16[8,80,512]{2,1,0:T(8,128)(2,1)}), bf16[8,80,512]{2,1,0:T(8,128)(2,1)S(1)}, u32[]{:S(2)}, u32[]{:S(2)}) async-start(bf16[8,80,512]{2,1,0:T(8,128)(2,1)} %bitcast.234), calls=%async_computation.3 | async-start | bytes 1310720 | tf_op jit(solution)/shard_map/all_to_all | solution.py:177
  176.3 47.3 %all-gather.10.cloned.1.call-start = ((), (), s32[]{:S(2)}) async-start(), calls=%async_computation.8 | async-start | bytes 1310720 | tf_op jit(solution)/shard_map/all_gather | solution.py:185
  176.3 6.7 %copy-start.37 = (f32[64,64]{1,0:T(8,128)}, f32[64,64]{1,0:T(8,128)S(1)}, u32[]{:S(2)}) copy-start(f32[64,64]{1,0:T(8,128)S(1)} %fusion.90) | copy-start | bytes 49156
  176.7 25.7 %copy-start.51 = (f32[8,32]{1,0:T(8,128)}, f32[8,32]{1,0:T(8,128)S(1)}, u32[]{:S(2)}) copy-start(f32[8,32]{1,0:T(8,128)S(1)} %get-tuple-element.68) | copy-start | bytes 3076
  176.7 27.0 %copy-start.45 = (f32[8,32]{1,0:T(8,128)}, f32[8,32]{1,0:T(8,128)S(1)}, u32[]{:S(2)}) copy-start(f32[8,32]{1,0:T(8,128)S(1)} %get-tuple-element.70) | copy-start | bytes 3076
  176.7 54.8 %copy-start.49 = (f32[8,32]{1,0:T(8,128)}, f32[8,32]{1,0:T(8,128)S(1)}, u32[]{:S(2)}) copy-start(f32[8,32]{1,0:T(8,128)S(1)} %get-tuple-element.67) | copy-start | bytes 3076
  194.4 2.2 copy-start.44
  196.4 4.8 %copy-start.36 = (f32[4,8,32]{2,0,1:T(4,128)S(1)}, f32[4,8,32]{2,0,1:T(4,128)}, u32[]{:S(2)}) copy-start(f32[4,8,32]{2,0,1:T(4,128)} %copy-done.35) | copy-start | bytes 12292
  199.1 122.8 %reduce-scatter.5.cloned.1.call-start = ((), (), s32[]{:S(2)}) async-start(), calls=%async_computation.9 | async-start | bytes 2359296 | tf_op jit(solution)/shard_map/reduce_scatter | solution.py:186
  205.5 5.2 %copy-start.27 = (bf16[640,512]{1,0:T(8,128)(2,1)S(1)}, bf16[640,512]{1,0:T(8,128)(2,1)}, u32[]{:S(2)}) copy-start(bf16[640,512]{1,0:T(8,128)(2,1)} %copy-done.26) | copy-start | bytes 1966084
  205.5 5.2 %copy-start.62 = (bf16[640,2048]{1,0:T(8,128)(2,1)S(1)}, bf16[640,2048]{1,0:T(8,128)(2,1)}, u32[]{:S(2)}) copy-start(bf16[640,2048]{1,0:T(8,128)(2,1)} %all-gather.6.cloned.1.call-done) | copy-start | bytes 7864324
  210.7 3.2 copy-start.63
  210.7 3.2 copy-start.64
  210.7 3.2 copy-start.65
  226.2 2.8 copy-start.3
  227.4 4.1 %copy-start.52 = (f32[8,32]{1,0:T(8,128)S(1)}, f32[8,32]{1,0:T(8,128)}, u32[]{:S(2)}) copy-start(f32[8,32]{1,0:T(8,128)} %copy-done.51) | copy-start | bytes 3076
  229.0 5.2 %copy-start.22 = (f32[1,8,32,64]{3,2,1,0:T(8,128)S(1)}, f32[1,8,32,64]{3,2,1,0:T(8,128)}, u32[]{:S(2)}) copy-start(f32[1,8,32,64]{3,2,1,0:T(8,128)} %get-tuple-element.76) | copy-start | bytes 196612
  231.5 4.5 %copy-start.17 = (f32[4,64,8,64]{3,1,2,0:T(8,128)S(1)}, f32[4,64,8,64]{3,1,2,0:T(8,128)}, u32[]{:S(2)}) copy-start(f32[4,64,8,64]{3,1,2,0:T(8,128)} %convolution_bitcast_fusion.1) | copy-start | bytes 1572868
  244.6 8.5 %copy-start.59 = (f32[256]{0:T(256)S(1)}, f32[256]{0:T(256)}, u32[]{:S(2)}) copy-start(f32[256]{0:T(256)} %exp.113) | copy-start | bytes 3076
  244.6 29.3 %copy-start.54 = (f32[8,256]{1,0:T(8,128)S(1)}, f32[8,256]{1,0:T(8,128)}, u32[]{:S(2)}) copy-start(f32[8,256]{1,0:T(8,128)} %fusion.23) | copy-start | bytes 24580
  246.6 27.4 %copy-start.23 = (f32[1,8,32,64]{3,2,1,0:T(8,128)}, f32[1,8,32,64]{3,2,1,0:T(8,128)S(1)}, u32[]{:S(2)}) copy-start(f32[1,8,32,64]{3,2,1,0:T(8,128)S(1)} %get-tuple-element.90) | copy-start | bytes 196612
  275.5 3.4 %copy-start.21 = (f32[4,8,64,32]{2,3,1,0:T(8,128)S(1)}, f32[4,8,64,32]{2,3,1,0:T(8,128)}, u32[]{:S(2)}) copy-start(f32[4,8,64,32]{2,3,1,0:T(8,128)} %fusion.28) | copy-start | bytes 786436
  278.9 4.6 %copy-start.13 = (f32[4,64,8,32]{1,3,2,0:T(8,128)}, f32[4,64,8,32]{1,3,2,0:T(8,128)S(1)}, u32[]{:S(2)}) copy-start(f32[4,64,8,32]{1,3,2,0:T(8,128)S(1)} %convolution_bitcast_fusion.2) | copy-start | bytes 786436
  278.9 1.8 copy-start.11
  278.9 1.8 copy-start.34
  278.9 1.8 copy-start.40
  280.7 2.7 copy-start.15
  283.4 12.9 %copy-start.5 = (f32[4,8,64,64]{3,2,1,0:T(8,128)S(1)}, f32[4,8,64,64]{3,2,1,0:T(8,128)}, u32[]{:S(2)}) copy-start(f32[4,8,64,64]{3,2,1,0:T(8,128)} %copy-done.4) | copy-start | bytes 1572868
  296.4 1.2 copy-start.7
  297.6 3.7 %copy-start.47 = (f32[4,8,32]{2,1,0:T(8,128)S(1)}, f32[4,8,32]{2,1,0:T(8,128)}, u32[]{:S(2)}) copy-start(f32[4,8,32]{2,1,0:T(8,128)} %get-tuple-element.84) | copy-start | bytes 12292
  297.6 4.7 %copy-start.56 = (f32[8,32]{1,0:T(8,128)S(1)}, f32[8,32]{1,0:T(8,128)}, u32[]{:S(2)}) copy-start(f32[8,32]{1,0:T(8,128)} %get-tuple-element.73) | copy-start | bytes 3076
  297.6 5.5 %copy-start.32 = (f32[8,32,64]{2,1,0:T(8,128)S(1)}, f32[8,32,64]{2,1,0:T(8,128)}, u32[]{:S(2)}) copy-start(f32[8,32,64]{2,1,0:T(8,128)} %bitcast_add_fusion.1) | copy-start | bytes 196612
  297.6 5.5 %copy-start.46 = (f32[8,32]{1,0:T(8,128)S(1)}, f32[8,32]{1,0:T(8,128)}, u32[]{:S(2)}) copy-start(f32[8,32]{1,0:T(8,128)} %copy-done.45) | copy-start | bytes 3076
  297.7 5.5 %copy-start.50 = (f32[8,32]{1,0:T(8,128)S(1)}, f32[8,32]{1,0:T(8,128)}, u32[]{:S(2)}) copy-start(f32[8,32]{1,0:T(8,128)} %copy-done.49) | copy-start | bytes 3076
  297.7 5.5 %copy-start.53 = (f32[8,32]{1,0:T(8,128)S(1)}, f32[8,32]{1,0:T(8,128)}, u32[]{:S(2)}) copy-start(f32[8,32]{1,0:T(8,128)} %copy-done.51) | copy-start | bytes 3076
  299.7 7.3 %copy-start.8 = (f32[4,64,8,32]{1,3,2,0:T(8,128)S(1)}, f32[4,64,8,32]{1,3,2,0:T(8,128)}, u32[]{:S(2)}) copy-start(f32[4,64,8,32]{1,3,2,0:T(8,128)} %get-tuple-element.82) | copy-start | bytes 786436
  300.2 12.4 %copy-start.29 = (f32[256,64]{0,1:T(8,128)S(1)}, f32[256,64]{0,1:T(8,128)}, u32[]{:S(2)}) copy-start(f32[256,64]{0,1:T(8,128)} %copy-done.28) | copy-start | bytes 196612
  300.3 12.4 %copy-start.30 = (f32[256,64]{0,1:T(8,128)S(1)}, f32[256,64]{0,1:T(8,128)}, u32[]{:S(2)}) copy-start(f32[256,64]{0,1:T(8,128)} %multiply_reduce_fusion) | copy-start | bytes 196612
  304.6 11.6 %copy-start.31 = (f32[1,1,8,32]{1,3,2,0:T(8,128)S(1)}, f32[1,1,8,32]{1,3,2,0:T(8,128)}, u32[]{:S(2)}) copy-start(f32[1,1,8,32]{1,3,2,0:T(8,128)} %copy.381) | copy-start | bytes 3076
  311.5 7.1 %copy-start.10 = (f32[4,64,8,32]{1,0,3,2:T(4,128)S(1)}, f32[4,64,8,32]{1,0,3,2:T(4,128)}, u32[]{:S(2)}) copy-start(f32[4,64,8,32]{1,0,3,2:T(4,128)} %copy-done.9) | copy-start | bytes 786436
  311.5 7.1 %copy-start.12 = (f32[4,64,8,32]{1,3,2,0:T(8,128)S(1)}, f32[4,64,8,32]{1,3,2,0:T(8,128)}, u32[]{:S(2)}) copy-start(f32[4,64,8,32]{1,3,2,0:T(8,128)} %convolution_bitcast_fusion.4) | copy-start | bytes 786436
  311.5 7.1 %copy-start.14 = (f32[4,64,8,32]{1,3,2,0:T(8,128)S(1)}, f32[4,64,8,32]{1,3,2,0:T(8,128)}, u32[]{:S(2)}) copy-start(f32[4,64,8,32]{1,3,2,0:T(8,128)} %copy-done.13) | copy-start | bytes 786436
  316.2 2.5 copy-start.16
  319.7 4.0 %copy-start.1 = (bf16[1,2048,512]{2,1,0:T(8,128)(2,1)S(1)}, bf16[1,2048,512]{2,1,0:T(8,128)(2,1)}, u32[]{:S(2)}) copy-start(bf16[1,2048,512]{2,1,0:T(8,128)(2,1)} %param.16) | copy-start | bytes 6291460
  (8 other events, 7.0 us)
Sparse Core Ops, SparseCore 0:
  42.1 38.3 all-gather.5
  82.2 39.3 all-gather.7
  132.0 39.5 reduce-scatter.2
  199.2 24.3 all-gather.9
  244.8 38.2 reduce-scatter.4
